TPU v7x, 512 devices: a whole 4x4x16 slice. The times are simulated.
512 devices in a mesh: sp: 16 (over z), dp: 32 (over y, x, core).
Axes of the slice: x: 4, y: 4, z: 16, core: 2. Of those that a mesh axis runs over, the one named last changes fastest.
Arguments:
- cotangent: bfloat16 [32, 2048, 2048], P('dp', 'sp'), may hold values from -6 to 6
- unit_pre: bfloat16 [32, 2048, 2048], P('dp', None, 'sp'), may hold values from -6 to 6
- gate_pre: bfloat16 [32, 2048, 2048], P('dp', None, 'sp'), may hold values from -15 to 15
- out_weight: bfloat16 [2048, 2048], P('dp', 'sp'), may hold values from -0.125 to 0.125
- mix_weight: bfloat16 [8, 128, 128], replicated, may hold values from -0.5 to 0.5
- mix_bias: bfloat16 [8, 128], replicated, may hold values from 0.099609375 to 1.8984375
- norm_gain: bfloat16 [2048], P('sp'), may hold values from 0.099609375 to 1.8984375
- norm_shift: bfloat16 [2048], P('sp'), may hold values from -3 to 3
Outputs:
- unit_grad: bfloat16 [32, 2048, 2048], P('dp', None, 'sp')
- gate_grad: bfloat16 [32, 2048, 2048], P('dp', None, 'sp')
- out_weight_grad: float32 [2048, 2048], P('dp', 'sp')
- mix_weight_grad: float32 [8, 128, 128], replicated
- mix_bias_grad: float32 [8, 128], replicated
- gain_grad: float32 [2048], P('sp')
- shift_grad: float32 [2048], P('sp')
All inputs are finite; a program needn't handle non-finite values.
Results may differ from a plain program's by a relative error of at most 0.015.
Values may be sent and summed in bfloat16 or wider, within the bound.
A program may use at most 64 MiB of HBM per device.

v0:
```python
import math
import jax
import jax.numpy as jnp
from jax import lax
from jax.sharding import PartitionSpec as P

GW = 2048
GROUPS = 8
BLK = 128
epsilon = 1e-05
tanh_coef = math.sqrt(2.0 / math.pi)


def sum_over(x, axis):
    devices = lax.axis_size(axis)
    copies = jnp.broadcast_to(x[None], (devices, *x.shape))
    return lax.all_to_all(copies, axis, 0, 0, tiled=True).sum(axis=0)


def gelu_slope(values):
    inner = tanh_coef * (values + 0.044715 * values * values * values)
    hyper = jnp.tanh(inner)
    return 0.5 * (1.0 + hyper) + 0.5 * values * (1.0 - hyper * hyper) * tanh_coef * (
        1.0 + 3.0 * 0.044715 * values * values
    )


def local(cotangent, unit_pre, gate_pre, out_weight, mix_weight, mix_bias, norm_gain, norm_shift):
    seq_len = unit_pre.shape[1]
    channels = unit_pre.shape[2]
    group_dim = GW // GROUPS
    blocks = seq_len // BLK
    sp_size = lax.axis_size("sp")
    sp_at = lax.axis_index("sp")
    group = sp_at * channels // group_dim
    weight_rows = lax.all_gather(out_weight, "sp", axis=1, tiled=True)
    weight_whole = lax.all_gather(weight_rows, "dp", axis=0, tiled=True)
    units = unit_pre[0].astype(jnp.float32)
    gates = gate_pre[0].astype(jnp.float32)
    unit_act = jax.nn.gelu(units)
    gate_act = jax.nn.gelu(gates)
    moments = sum_over(
        jnp.stack([jnp.sum(gate_act, axis=-1), jnp.sum(gate_act * gate_act, axis=-1)]), "sp"
    )
    mean_val = moments[0] / GW
    var_val = moments[1] / GW - mean_val * mean_val
    rstd_val = lax.rsqrt(var_val + epsilon)
    centred = (gate_act - mean_val[:, None]) * rstd_val[:, None]
    gain_vec = norm_gain.astype(jnp.float32)
    normed = (centred * gain_vec + norm_shift.astype(jnp.float32)).astype(jnp.bfloat16)
    causal = jnp.arange(BLK)[:, None] >= jnp.arange(BLK)[None, :]
    local_weight = lax.dynamic_index_in_dim(mix_weight, group, 0, keepdims=False)
    masked = jnp.where(causal, local_weight, jnp.zeros_like(local_weight))
    local_bias = lax.dynamic_index_in_dim(mix_bias, group, 0, keepdims=False).astype(jnp.float32)
    normed_blocks = normed.reshape(blocks, BLK, channels)
    mixed = jnp.einsum("ts,nsd->ntd", masked, normed_blocks, preferred_element_type=jnp.float32)
    mixed = (mixed + local_bias[None, :, None]).reshape(seq_len, channels)
    gated = (unit_act * mixed).astype(jnp.bfloat16)
    gated_rows = lax.all_to_all(gated, "sp", split_axis=0, concat_axis=1, tiled=True)
    head_rows = jnp.dot(cotangent[0], weight_whole, preferred_element_type=jnp.float32)
    head = lax.all_to_all(
        head_rows.astype(jnp.bfloat16), "sp", split_axis=1, concat_axis=0, tiled=True
    ).astype(jnp.float32)
    weight_part = lax.dot_general(
        cotangent[0], gated_rows, (((0,), (0,)), ((), ())), preferred_element_type=jnp.float32
    ).astype(jnp.bfloat16)
    token_count = lax.axis_size("dp") * seq_len
    norm_scale = 1.0 / math.sqrt(token_count)
    mix_scale = 1.0 / math.sqrt(token_count // BLK * group_dim)
    plane_sum = lax.psum_scatter(weight_part, "dp", scatter_dimension=0, tiled=True)
    plane_parts = jnp.moveaxis(plane_sum.reshape(plane_sum.shape[0], sp_size, channels), 1, 0)
    arrived = lax.all_to_all(plane_parts, "sp", split_axis=0, concat_axis=0, tiled=True)
    out_grad = arrived.astype(jnp.float32).sum(axis=0) * norm_scale
    unit_grad = (head * mixed * gelu_slope(units)).astype(jnp.bfloat16)
    mix_grad = head * unit_act
    mix_round = mix_grad.astype(jnp.bfloat16).reshape(blocks, BLK, channels)
    mix_term = jnp.einsum(
        "ntd,nsd->ts", mix_round, normed_blocks, preferred_element_type=jnp.float32
    )
    mix_term = jnp.where(causal, mix_term, jnp.float32(0.0))
    bias_term = jnp.sum(mix_grad.reshape(blocks, BLK, channels), axis=(0, 2))
    normed_grad = jnp.einsum(
        "ts,ntd->nsd", masked, mix_round, preferred_element_type=jnp.float32
    ).reshape(seq_len, channels)
    gain_term = jnp.sum(normed_grad * centred, axis=0)
    shift_term = jnp.sum(normed_grad, axis=0)
    scaled = normed_grad * gain_vec
    back_sums = sum_over(
        jnp.stack([jnp.sum(scaled, axis=-1), jnp.sum(scaled * centred, axis=-1)]), "sp"
    )
    first_m = back_sums[0] / GW
    second_m = back_sums[1] / GW
    gate_grad = (
        rstd_val[:, None]
        * (scaled - first_m[:, None] - centred * second_m[:, None])
        * gelu_slope(gates)
    ).astype(jnp.bfloat16)
    group_hot = (jnp.arange(GROUPS) == group).astype(jnp.float32)
    own_hot = (jnp.arange(sp_size) == sp_at).astype(jnp.float32)
    packed = jnp.concatenate(
        [
            (group_hot[:, None, None] * mix_term).reshape(GROUPS * BLK, BLK),
            group_hot[:, None] * bias_term,
            own_hot[:, None] * gain_term,
            own_hot[:, None] * shift_term,
        ]
    )
    total = lax.psum(packed, ("sp", "dp"))
    top = GROUPS * BLK
    weight_total = total[:top].reshape(GROUPS, BLK, BLK)
    bias_total = total[top : top + GROUPS]
    tail = total[top + GROUPS :]
    gain_total = lax.dynamic_index_in_dim(tail, sp_at, 0, keepdims=False)
    shift_total = lax.dynamic_index_in_dim(tail, sp_size + sp_at, 0, keepdims=False)
    return (
        unit_grad[None],
        gate_grad[None],
        out_grad,
        weight_total * mix_scale,
        bias_total * mix_scale,
        gain_total * norm_scale,
        shift_total * norm_scale,
    )


def solution(mesh):
    return jax.shard_map(
        local,
        mesh=mesh,
        in_specs=(
            P("dp", "sp", None),
            P("dp", None, "sp"),
            P("dp", None, "sp"),
            P("dp", "sp"),
            P(),
            P(),
            P("sp"),
            P("sp"),
        ),
        out_specs=(
            P("dp", None, "sp"),
            P("dp", None, "sp"),
            P("dp", "sp"),
            P(),
            P(),
            P("sp"),
            P("sp"),
        ),
        check_vma=False,
    )
```

profile of v0, /device:TPU:32, one launch (start us, length us, event | category | flops | bytes accessed | tf_op | source)
XLA Modules:
  0.0 828.7 jit_solution(9951408123859522207)
XLA Ops:
  7.2 0.0 all-gather.2.cloned.1.call-start
  7.2 37.3 %all_gather.6 = bf16[64,2048]{1,0:T(8,128)(2,1)} all-gather(bf16[64,128]{1,0:T(8,128)(2,1)} %param.11), channel_id=1, replica_groups=mesh['sp'=16,'dp'=32] {'sp'}, dimensions={1}, use_global_device_ids=true | all-gather | bytes 278528 | tf_op jit(solution)/shard_map/all_gather | solution.py:36
  44.6 0.0 all-gather.2.cloned.1.call-update
  44.6 1.8 fusion.58
  46.4 0.8 broadcast_in_dim.11
  47.2 8.9 %all-to-all-start.1 = ((f32[16,2,2048]{2,1,0:T(2,128)}), f32[16,2,2048]{2,1,0:T(2,128)S(1)}, u32[]{:S(2)}, u32[]{:S(2)}) async-start(f32[16,2,2048]{2,1,0:T(2,128)} %broadcast_in_dim.11), calls=%async_computation.1 | async-start | bytes 524288 | tf_op jit(solution)/shard_map/all_to_all | solution.py:17
  56.1 54.5 %all-gather.2.cloned.1.call-done = bf16[2048,2048]{1,0:T(8,128)(2,1)} async-done(((bf16[64,2048]{1,0:T(8,128)(2,1)}), bf16[2048,2048]{1,0:T(8,128)(2,1)}) %all-gather.2.cloned.1.call-update) | async-done | bytes 8388624 | tf_op jit(solution)/shard_map/all_gather | solution.py:37
  110.6 4.6 fusion.5
  115.3 0.9 copy.53
  116.2 12.7 %all-to-all-start = ((bf16[128,16,128]{2,0,1:T(8,128)(2,1)}), bf16[128,16,128]{2,0,1:T(8,128)(2,1)S(1)}, u32[]{:S(2)}, u32[]{:S(2)}) async-start(bf16[128,16,128]{2,0,1:T(8,128)(2,1)} %bitcast.135), calls=%async_computation | async-start | bytes 1048576 | tf_op jit(solution)/shard_map/all_to_all | solution.py:61
  128.9 0.1 reduce_sum.92
  129.0 29.5 %all-to-all-done = bf16[128,16,128]{2,0,1:T(8,128)(2,1)S(1)} async-done(((bf16[128,16,128]{2,0,1:T(8,128)(2,1)}), bf16[128,16,128]{2,0,1:T(8,128)(2,1)S(1)}, u32[]{:S(2)}, u32[]{:S(2)}) %all-to-all-start) | async-done | bytes 524320 | tf_op jit(solution)/shard_map/all_to_all | solution.py:61
  158.6 0.5 fusion.59
  159.1 1.0 copy-done.3
  160.1 3.3 fusion.56
  163.4 0.8 broadcast_in_dim.15
  164.2 6.1 all-to-all-start.2
  170.3 0.7 fusion.80
  171.0 17.5 %all-to-all-done.2 = f32[16,2,2048]{2,1,0:T(2,128)S(1)} async-done(((f32[16,2,2048]{2,1,0:T(2,128)}), f32[16,2,2048]{2,1,0:T(2,128)S(1)}, u32[]{:S(2)}, u32[]{:S(2)}) %all-to-all-start.2) | async-done | bytes 262176 | tf_op jit(solution)/shard_map/all_to_all | solution.py:17
  188.6 0.1 reduce_sum.95
  188.7 2.8 fusion.51
  191.5 3.0 multiply_convert_fusion
  194.4 6.1 all-to-all-start.3
  200.5 0.0 all-reduce.2.cloned.1.call-start
  200.6 0.3 reduce_sum.99
  200.8 0.1 broadcast_bitcast_fusion
  200.9 2.5 fusion.6
  203.5 0.2 bitcast_multiply_fusion.5
  203.7 0.1 broadcast_multiply_fusion.2
  203.7 0.8 pad_maximum_fusion
  204.6 0.0 reduce-scatter.4.cloned.1.call-start
  204.6 24.2 %all-to-all-done.3 = bf16[16,128,128]{2,1,0:T(8,128)(2,1)S(1)} async-done(((bf16[16,128,128]{2,1,0:T(8,128)(2,1)}), bf16[16,128,128]{2,1,0:T(8,128)(2,1)S(1)}, u32[]{:S(2)}, u32[]{:S(2)}) %all-to-all-start.3) | async-done | bytes 524320 | tf_op jit(solution)/shard_map/all_to_all | solution.py:59
  228.9 0.3 copy.36
  229.2 5.5 convert_bitcast_fusion
  234.7 12.4 %copy.42 = bf16[2048,2048]{1,0:T(8,128)(2,1)} copy(bf16[2048,2048]{0,1:T(8,128)(2,1)} %convert_bitcast_fusion) | data formatting | bytes 16777216
  247.1 423.4 %all-reduce.2.cloned.1.call-done = f32[1064,128]{1,0:T(8,128)} async-done(((f32[1064,128]{1,0:T(8,128)}), f32[1064,128]{1,0:T(8,128)}) %all-reduce.2.cloned.1.call-update) | async-done | bytes 544784 | tf_op jit(solution)/shard_map/psum | solution.py:108
  670.5 0.7 slice.34
  671.2 117.9 %reduce-scatter.4.cloned.1.call-done = bf16[64,2048]{1,0:T(8,128)(2,1)} async-done(((bf16[2048,2048]{1,0:T(8,128)(2,1)}), bf16[64,2048]{1,0:T(8,128)(2,1)}) %reduce-scatter.4.cloned.1.call-update) | async-done | bytes 262160
  789.1 1.2 copy.43
  790.4 0.9 copy.37
  791.3 12.7 %all-to-all-start.4 = ((bf16[16,64,128]{2,1,0:T(8,128)(2,1)}), bf16[16,64,128]{2,1,0:T(8,128)(2,1)S(1)}, u32[]{:S(2)}, u32[]{:S(2)}) async-start(bf16[16,64,128]{2,1,0:T(8,128)(2,1)} %bitcast.29), calls=%async_computation.4 | async-start | bytes 524288 | tf_op jit(solution)/shard_map/all_to_all | solution.py:72
  803.9 0.5 fusion.84
  804.5 1.3 slice_multiply_fusion.5
  805.7 1.9 slice_multiply_fusion
  807.6 1.5 fusion.30
  809.1 12.2 %all-to-all-done.4 = bf16[16,64,128]{2,1,0:T(8,128)(2,1)S(1)} async-done(((bf16[16,64,128]{2,1,0:T(8,128)(2,1)}), bf16[16,64,128]{2,1,0:T(8,128)(2,1)S(1)}, u32[]{:S(2)}, u32[]{:S(2)}) %all-to-all-start.4) | async-done | bytes 262176 | tf_op jit(solution)/shard_map/all_to_all | solution.py:72
  821.3 0.1 copy.46
  821.4 0.7 copy.39
  (28 shorter events, 0.2 us)
Async XLA Ops:
  7.2 103.5 %copy-start = (bf16[1,128,2048]{2,1,0:T(8,128)(2,1)S(1)}, bf16[1,128,2048]{2,1,0:T(8,128)(2,1)}, u32[]{:S(2)}) copy-start(bf16[1,128,2048]{2,1,0:T(8,128)(2,1)} %param.8) | copy-start | bytes 1572868
  7.2 103.4 %all-gather.2.cloned.1.call-start = ((), (), s32[]{:S(2)}) async-start(), calls=%async_computation.6 | async-start | bytes 8650752 | tf_op jit(solution)/shard_map/all_gather | solution.py:37
  47.2 69.0 %all-to-all-start.1 = ((f32[16,2,2048]{2,1,0:T(2,128)}), f32[16,2,2048]{2,1,0:T(2,128)S(1)}, u32[]{:S(2)}, u32[]{:S(2)}) async-start(f32[16,2,2048]{2,1,0:T(2,128)} %broadcast_in_dim.11), calls=%async_computation.1 | async-start | bytes 524288 | tf_op jit(solution)/shard_map/all_to_all | solution.py:17
  56.1 72.8 %copy-start.5 = (bf16[128]{0:T(256)(128)(2,1)S(1)}, bf16[128]{0:T(256)(128)(2,1)}, u32[]{:S(2)}) copy-start(bf16[128]{0:T(256)(128)(2,1)} %param.14) | copy-start | bytes 772
  56.1 102.5 %copy-start.2 = (bf16[1,2048,128]{2,1,0:T(8,128)(2,1)S(1)}, bf16[1,2048,128]{2,1,0:T(8,128)(2,1)}, u32[]{:S(2)}) copy-start(bf16[1,2048,128]{2,1,0:T(8,128)(2,1)} %param.9) | copy-start | bytes 1572868
  56.1 104.0 %copy-start.1 = (bf16[1,2048,128]{2,1,0:T(8,128)(2,1)S(1)}, bf16[1,2048,128]{2,1,0:T(8,128)(2,1)}, u32[]{:S(2)}) copy-start(bf16[1,2048,128]{2,1,0:T(8,128)(2,1)} %param.10) | copy-start | bytes 1572868
  115.3 55.1 %copy-start.6 = (bf16[128]{0:T(256)(128)(2,1)S(1)}, bf16[128]{0:T(256)(128)(2,1)}, u32[]{:S(2)}) copy-start(bf16[128]{0:T(256)(128)(2,1)} %param.15) | copy-start | bytes 772
  116.2 42.4 %all-to-all-start = ((bf16[128,16,128]{2,0,1:T(8,128)(2,1)}), bf16[128,16,128]{2,0,1:T(8,128)(2,1)S(1)}, u32[]{:S(2)}, u32[]{:S(2)}) async-start(bf16[128,16,128]{2,0,1:T(8,128)(2,1)} %bitcast.135), calls=%async_computation | async-start | bytes 1048576 | tf_op jit(solution)/shard_map/all_to_all | solution.py:61
  159.1 1.0 copy-start.3
  164.2 24.4 %all-to-all-start.2 = ((f32[16,2,2048]{2,1,0:T(2,128)}), f32[16,2,2048]{2,1,0:T(2,128)S(1)}, u32[]{:S(2)}, u32[]{:S(2)}) async-start(f32[16,2,2048]{2,1,0:T(2,128)} %broadcast_in_dim.15), calls=%async_computation.2 | async-start | bytes 524288 | tf_op jit(solution)/shard_map/all_to_all | solution.py:17
  194.4 34.5 %all-to-all-start.3 = ((bf16[16,128,128]{2,1,0:T(8,128)(2,1)}), bf16[16,128,128]{2,1,0:T(8,128)(2,1)S(1)}, u32[]{:S(2)}, u32[]{:S(2)}) async-start(bf16[16,128,128]{2,1,0:T(8,128)(2,1)} %get-tuple-element.36), calls=%async_computation.3 | async-start | bytes 1048576 | tf_op jit(solution)/shard_map/all_to_all | solution.py:59
  200.5 470.0 %all-reduce.2.cloned.1.call-start = ((), (), s32[]{:S(2)}) async-start(), calls=%async_computation.7 | async-start | bytes 1089536 | tf_op jit(solution)/shard_map/psum | solution.py:108
  204.6 584.5 %reduce-scatter.4.cloned.1.call-start = ((), (), s32[]{:S(2)}) async-start(), calls=%async_computation.8 | async-start | bytes 8650752
  247.1 560.5 %copy-start.4 = (f32[16,128,128]{2,1,0:T(8,128)S(1)}, f32[16,128,128]{2,1,0:T(8,128)}, u32[]{:S(2)}) copy-start(f32[16,128,128]{2,1,0:T(8,128)} %get-tuple-element.37) | copy-start | bytes 3145732
  791.3 30.0 %all-to-all-start.4 = ((bf16[16,64,128]{2,1,0:T(8,128)(2,1)}), bf16[16,64,128]{2,1,0:T(8,128)(2,1)S(1)}, u32[]{:S(2)}, u32[]{:S(2)}) async-start(bf16[16,64,128]{2,1,0:T(8,128)(2,1)} %bitcast.29), calls=%async_computation.4 | async-start | bytes 524288 | tf_op jit(solution)/shard_map/all_to_all | solution.py:72
Sparse Core Ops, SparseCore 0:
  44.7 65.8 all-gather.1
  206.8 463.6 all-reduce.1
  675.1 114.0 reduce-scatter.3
where the time goes:
time: 830 us; the launch traced here: 829 us
  waiting for transfers between devices  679 us (82%)
  starting transfers between devices  46.6 us (6%)
  blocking collectives  37.3 us (4%)
  local copies, waits for them, and re-layouts  19.8 us (2%)
  matrix products  18.9 us (2%)
  between operations  13.9 us (2%)
  other arithmetic  12.7 us (2%)
    psum x1, waiting for transfers between devices, local(): total = lax.psum(packed, ('sp', 'dp'))  423 us
    unnamed x4, waiting for transfers between devices  118 us
    all_gather x1, waiting for transfers between devices, local(): weight_whole = lax.all_gather(weight_rows, 'dp', axis=0, tiled=True)  54.5 us
    all_gather x1, blocking collectives, local(): weight_rows = lax.all_gather(out_weight, 'sp', axis=1, tiled=True)  37.3 us
    all_to_all x1, waiting for transfers between devices, local(): lax.all_to_all(head_rows.astype(jnp.bfloat16), 'sp', split_axis=1, concat...  29.5 us
    all_to_all x1, waiting for transfers between devices, local(): lax.all_to_all(gated, 'sp', split_axis=0, concat_axis=1, tiled=True)  24.2 us
    all_to_all x2, waiting for transfers between devices, sum_over(): return lax.all_to_all(copies, axis, 0, 0, tiled=True).sum(axis=0)  17.5 us
  transfers between devices with their start and end apart: 8, of which 7 were waited for; matrix products, arithmetic and copies ran while one was open for 4% of the time, Pallas kernels for 0%

commit v1 on v0

--- a/solution.py
+++ b/solution.py
@@ -34,7 +34,9 @@
     sp_at = lax.axis_index("sp")
     group = sp_at * channels // group_dim
     weight_rows = lax.all_gather(out_weight, "sp", axis=1, tiled=True)
-    weight_whole = lax.all_gather(weight_rows, "dp", axis=0, tiled=True)
+    weight_whole = jnp.concatenate(
+        lax.all_to_all(jnp.stack([weight_rows] * lax.axis_size("dp")), "dp", 0, 0), axis=0
+    )
     units = unit_pre[0].astype(jnp.float32)
     gates = gate_pre[0].astype(jnp.float32)
     unit_act = jax.nn.gelu(units)

time: 830 us -> 774 us (0.933)
  the two profiles are of different devices: /device:TPU:32 before, /device:TPU:1 now
where the time goes in v1:
time: 774 us; the launch traced here: 773 us
  waiting for transfers between devices  611 us (79%)
  starting transfers between devices  60.3 us (8%)
  blocking collectives  30.8 us (4%)
  local copies, waits for them, and re-layouts  24.1 us (3%)
  matrix products  19 us (2%)
  between operations  15.7 us (2%)
  other arithmetic  11.7 us (2%)
    psum x1, waiting for transfers between devices, local(): total = lax.psum(packed, ('sp', 'dp'))  442 us
    all_to_all x1, waiting for transfers between devices, local(): lax.all_to_all(jnp.stack([weight_rows] * lax.axis_size('dp')), 'dp', 0, 0)  99.9 us
    all_gather x1, blocking collectives, local(): weight_rows = lax.all_gather(out_weight, 'sp', axis=1, tiled=True)  30.8 us
    all_to_all x2, starting transfers between devices, sum_over(): return lax.all_to_all(copies, axis, 0, 0, tiled=True).sum(axis=0)  20 us
    all_to_all x2, waiting for transfers between devices, sum_over(): return lax.all_to_all(copies, axis, 0, 0, tiled=True).sum(axis=0)  19 us
    all_to_all x1, waiting for transfers between devices, local(): lax.all_to_all(head_rows.astype(jnp.bfloat16), 'sp', split_axis=1, concat...  18.7 us
    all_to_all x1, waiting for transfers between devices, local(): lax.all_to_all(gated, 'sp', split_axis=0, concat_axis=1, tiled=True)  18.1 us
  transfers between devices with their start and end apart: 8, of which 7 were waited for; matrix products, arithmetic and copies ran while one was open for 5% of the time, Pallas kernels for 0%

profile of v1, /device:TPU:1, one launch (start us, length us, event | category | flops | bytes accessed | tf_op | source)
XLA Modules:
  0.0 772.6 jit_solution(18408277422260110638)
XLA Ops:
  8.0 30.8 %all_gather.3 = bf16[64,2048]{1,0:T(8,128)(2,1)S(1)} all-gather(bf16[64,128]{1,0:T(8,128)(2,1)} %param.11), channel_id=1, replica_groups=mesh['sp'=16,'dp'=32] {'sp'}, dimensions={1}, use_global_device_ids=true | all-gather | bytes 278528 | tf_op jit(solution)/shard_map/all_gather | solution.py:36
  38.8 4.3 stack.14
  43.1 15.1 %all-to-all-start = ((bf16[32,64,2048]{2,1,0:T(8,128)(2,1)}), bf16[32,64,2048]{2,1,0:T(8,128)(2,1)}, u32[]{:S(2)}, u32[]{:S(2)}) async-start(bf16[32,64,2048]{2,1,0:T(8,128)(2,1)} %stack.14), calls=%async_computation | async-start | bytes 16777216 | tf_op jit(solution)/shard_map/all_to_all | solution.py:38
  58.2 0.7 fusion.58
  59.0 99.9 %all-to-all-done = bf16[32,64,2048]{2,1,0:T(8,128)(2,1)} async-done(((bf16[32,64,2048]{2,1,0:T(8,128)(2,1)}), bf16[32,64,2048]{2,1,0:T(8,128)(2,1)}, u32[]{:S(2)}, u32[]{:S(2)}) %all-to-all-start) | async-done | bytes 8388640 | tf_op jit(solution)/shard_map/all_to_all | solution.py:38
  158.9 0.8 broadcast_in_dim.11
  159.7 6.5 all-to-all-start.2
  166.2 4.7 fusion.5
  171.0 0.9 copy.53
  171.9 7.0 all-to-all-done.2
  178.9 6.1 all-to-all-start.1
  185.1 0.1 reduce_sum.92
  185.2 18.7 %all-to-all-done.1 = bf16[128,16,128]{2,0,1:T(8,128)(2,1)S(1)} async-done(((bf16[128,16,128]{2,0,1:T(8,128)(2,1)}), bf16[128,16,128]{2,0,1:T(8,128)(2,1)S(1)}, u32[]{:S(2)}, u32[]{:S(2)}) %all-to-all-start.1) | async-done | bytes 524320 | tf_op jit(solution)/shard_map/all_to_all | solution.py:63
  203.9 0.5 fusion.59
  204.4 1.0 copy-done.3
  205.4 3.3 fusion.56
  208.7 0.8 broadcast_in_dim.15
  209.5 13.5 %all-to-all-start.3 = ((f32[16,2,2048]{2,1,0:T(2,128)}), f32[16,2,2048]{2,1,0:T(2,128)S(1)}, u32[]{:S(2)}, u32[]{:S(2)}) async-start(f32[16,2,2048]{2,1,0:T(2,128)} %broadcast_in_dim.15), calls=%async_computation.3 | async-start | bytes 524288 | tf_op jit(solution)/shard_map/all_to_all | solution.py:17
  223.1 0.7 fusion.80
  223.8 12.0 %all-to-all-done.3 = f32[16,2,2048]{2,1,0:T(2,128)S(1)} async-done(((f32[16,2,2048]{2,1,0:T(2,128)}), f32[16,2,2048]{2,1,0:T(2,128)S(1)}, u32[]{:S(2)}, u32[]{:S(2)}) %all-to-all-start.3) | async-done | bytes 262176 | tf_op jit(solution)/shard_map/all_to_all | solution.py:17
  235.8 0.1 reduce_sum.95
  235.9 2.8 fusion.51
  238.7 3.0 multiply_convert_fusion
  241.6 9.1 %all-to-all-start.4 = ((bf16[16,128,128]{2,1,0:T(8,128)(2,1)}), bf16[16,128,128]{2,1,0:T(8,128)(2,1)S(1)}, u32[]{:S(2)}, u32[]{:S(2)}) async-start(bf16[16,128,128]{2,1,0:T(8,128)(2,1)} %get-tuple-element.36), calls=%async_computation.4 | async-start | bytes 1048576 | tf_op jit(solution)/shard_map/all_to_all | solution.py:61
  250.7 0.0 all-reduce.2.cloned.1.call-start
  250.8 0.3 reduce_sum.99
  251.1 0.1 broadcast_bitcast_fusion
  251.1 2.5 fusion.6
  253.7 0.2 bitcast_multiply_fusion.5
  253.9 0.1 broadcast_multiply_fusion.2
  254.0 0.8 pad_maximum_fusion
  254.8 0.2 reduce-scatter.4.cloned.1.call-start
  255.1 18.1 %all-to-all-done.4 = bf16[16,128,128]{2,1,0:T(8,128)(2,1)S(1)} async-done(((bf16[16,128,128]{2,1,0:T(8,128)(2,1)}), bf16[16,128,128]{2,1,0:T(8,128)(2,1)S(1)}, u32[]{:S(2)}, u32[]{:S(2)}) %all-to-all-start.4) | async-done | bytes 524320 | tf_op jit(solution)/shard_map/all_to_all | solution.py:61
  273.2 0.3 copy.36
  273.5 5.5 convert_bitcast_fusion
  279.0 12.3 %copy.42 = bf16[2048,2048]{1,0:T(8,128)(2,1)} copy(bf16[2048,2048]{0,1:T(8,128)(2,1)} %convert_bitcast_fusion) | data formatting | bytes 16777216
  291.4 442.4 %all-reduce.2.cloned.1.call-done = f32[1064,128]{1,0:T(8,128)} async-done(((f32[1064,128]{1,0:T(8,128)}), f32[1064,128]{1,0:T(8,128)}) %all-reduce.2.cloned.1.call-update) | async-done | bytes 544784 | tf_op jit(solution)/shard_map/psum | solution.py:110
  733.8 0.7 slice.34
  734.5 1.2 copy.43
  735.7 0.9 copy.37
  736.6 9.8 %all-to-all-start.5 = ((bf16[16,64,128]{2,1,0:T(8,128)(2,1)}), bf16[16,64,128]{2,1,0:T(8,128)(2,1)S(1)}, u32[]{:S(2)}, u32[]{:S(2)}) async-start(bf16[16,64,128]{2,1,0:T(8,128)(2,1)} %bitcast.30), calls=%async_computation.5 | async-start | bytes 524288 | tf_op jit(solution)/shard_map/all_to_all | solution.py:74
  746.4 0.5 fusion.84
  746.9 1.3 slice_multiply_fusion.5
  748.2 1.9 slice_multiply_fusion
  750.1 1.5 fusion.30
  751.6 12.7 %all-to-all-done.5 = bf16[16,64,128]{2,1,0:T(8,128)(2,1)S(1)} async-done(((bf16[16,64,128]{2,1,0:T(8,128)(2,1)}), bf16[16,64,128]{2,1,0:T(8,128)(2,1)S(1)}, u32[]{:S(2)}, u32[]{:S(2)}) %all-to-all-start.5) | async-done | bytes 262176 | tf_op jit(solution)/shard_map/all_to_all | solution.py:74
  764.3 0.1 copy.46
  764.4 0.7 copy.39
  (28 shorter events, 0.2 us)
Async XLA Ops:
  8.0 158.2 %copy-start = (bf16[1,128,2048]{2,1,0:T(8,128)(2,1)S(1)}, bf16[1,128,2048]{2,1,0:T(8,128)(2,1)}, u32[]{:S(2)}) copy-start(bf16[1,128,2048]{2,1,0:T(8,128)(2,1)} %param.8) | copy-start | bytes 1572868
  43.1 15.1 %copy-start.1 = (bf16[1,2048,128]{2,1,0:T(8,128)(2,1)S(1)}, bf16[1,2048,128]{2,1,0:T(8,128)(2,1)}, u32[]{:S(2)}) copy-start(bf16[1,2048,128]{2,1,0:T(8,128)(2,1)} %param.10) | copy-start | bytes 1572868
  43.1 115.8 %all-to-all-start = ((bf16[32,64,2048]{2,1,0:T(8,128)(2,1)}), bf16[32,64,2048]{2,1,0:T(8,128)(2,1)}, u32[]{:S(2)}, u32[]{:S(2)}) async-start(bf16[32,64,2048]{2,1,0:T(8,128)(2,1)} %stack.14), calls=%async_computation | async-start | bytes 16777216 | tf_op jit(solution)/shard_map/all_to_all | solution.py:38
  159.7 19.2 %all-to-all-start.2 = ((f32[16,2,2048]{2,1,0:T(2,128)}), f32[16,2,2048]{2,1,0:T(2,128)S(1)}, u32[]{:S(2)}, u32[]{:S(2)}) async-start(f32[16,2,2048]{2,1,0:T(2,128)} %broadcast_in_dim.11), calls=%async_computation.2 | async-start | bytes 524288 | tf_op jit(solution)/shard_map/all_to_all | solution.py:17
  166.2 18.8 %copy-start.5 = (bf16[128]{0:T(256)(128)(2,1)S(1)}, bf16[128]{0:T(256)(128)(2,1)}, u32[]{:S(2)}) copy-start(bf16[128]{0:T(256)(128)(2,1)} %param.14) | copy-start | bytes 772
  166.2 37.6 %copy-start.2 = (bf16[1,2048,128]{2,1,0:T(8,128)(2,1)S(1)}, bf16[1,2048,128]{2,1,0:T(8,128)(2,1)}, u32[]{:S(2)}) copy-start(bf16[1,2048,128]{2,1,0:T(8,128)(2,1)} %param.9) | copy-start | bytes 1572868
  171.0 52.1 %copy-start.6 = (bf16[128]{0:T(256)(128)(2,1)S(1)}, bf16[128]{0:T(256)(128)(2,1)}, u32[]{:S(2)}) copy-start(bf16[128]{0:T(256)(128)(2,1)} %param.15) | copy-start | bytes 772
  178.9 24.9 %all-to-all-start.1 = ((bf16[128,16,128]{2,0,1:T(8,128)(2,1)}), bf16[128,16,128]{2,0,1:T(8,128)(2,1)S(1)}, u32[]{:S(2)}, u32[]{:S(2)}) async-start(bf16[128,16,128]{2,0,1:T(8,128)(2,1)} %bitcast.136), calls=%async_computation.1 | async-start | bytes 1048576 | tf_op jit(solution)/shard_map/all_to_all | solution.py:63
  204.4 1.0 copy-start.3
  209.5 26.3 %all-to-all-start.3 = ((f32[16,2,2048]{2,1,0:T(2,128)}), f32[16,2,2048]{2,1,0:T(2,128)S(1)}, u32[]{:S(2)}, u32[]{:S(2)}) async-start(f32[16,2,2048]{2,1,0:T(2,128)} %broadcast_in_dim.15), calls=%async_computation.3 | async-start | bytes 524288 | tf_op jit(solution)/shard_map/all_to_all | solution.py:17
  241.6 31.6 %all-to-all-start.4 = ((bf16[16,128,128]{2,1,0:T(8,128)(2,1)}), bf16[16,128,128]{2,1,0:T(8,128)(2,1)S(1)}, u32[]{:S(2)}, u32[]{:S(2)}) async-start(bf16[16,128,128]{2,1,0:T(8,128)(2,1)} %get-tuple-element.36), calls=%async_computation.4 | async-start | bytes 1048576 | tf_op jit(solution)/shard_map/all_to_all | solution.py:61
  250.7 483.1 %all-reduce.2.cloned.1.call-start = ((), (), s32[]{:S(2)}) async-start(), calls=%async_computation.7 | async-start | bytes 1089536 | tf_op jit(solution)/shard_map/psum | solution.py:110
  254.8 479.7 %reduce-scatter.4.cloned.1.call-start = ((), (), s32[]{:S(2)}) async-start(), calls=%async_computation.8 | async-start | bytes 8650752
  291.3 458.8 %copy-start.4 = (f32[16,128,128]{2,1,0:T(8,128)S(1)}, f32[16,128,128]{2,1,0:T(8,128)}, u32[]{:S(2)}) copy-start(f32[16,128,128]{2,1,0:T(8,128)} %get-tuple-element.37) | copy-start | bytes 3145732
  736.6 27.6 %all-to-all-start.5 = ((bf16[16,64,128]{2,1,0:T(8,128)(2,1)}), bf16[16,64,128]{2,1,0:T(8,128)(2,1)S(1)}, u32[]{:S(2)}, u32[]{:S(2)}) async-start(bf16[16,64,128]{2,1,0:T(8,128)(2,1)} %bitcast.30), calls=%async_computation.5 | async-start | bytes 524288 | tf_op jit(solution)/shard_map/all_to_all | solution.py:74
Sparse Core Ops, SparseCore 0:
  257.0 476.7 all-reduce.1
Sparse Core Ops, SparseCore 1:
  291.4 125.9 reduce-scatter.3
